TPU v7x, 32 devices: a whole 2x2x4 slice. The times are simulated.
32 devices in a mesh: rep: 2 (over x), fs: 8 (over z, y), tp: 2 (over core).
Axes of the slice: x: 2, y: 2, z: 4, core: 2. Of those that a mesh axis runs over, the one named last changes fastest.
Arguments:
- tokens: bfloat16 [16384, 2048], P(('rep', 'fs'), 'tp'), may hold values from -6 to 6
- attention_pre_gain: float32 [2048], replicated, may hold values from 0.1 to 1.9
- query_matrix: bfloat16 [2048, 512], P('fs', 'tp'), may hold values from -0.125 to 0.125
- key_matrix: bfloat16 [2048, 512], P('fs', 'tp'), may hold values from -0.125 to 0.125
- value_matrix: bfloat16 [2048, 1024], P('fs', 'tp'), may hold values from -0.125 to 0.125
- decay_first_weight: bfloat16 [2048, 16], replicated, may hold values from -0.125 to 0.125
- decay_second_weight: bfloat16 [16, 512], P(None, 'tp'), may hold values from -1.5 to 1.5
- decay_offset_bias: float32 [512], P('tp'), may hold values from 0 to 6
- extra_log_surge: float32 [16384, 2], P(('rep', 'fs'), 'tp'), may hold values from -0.7 to 0
- readout_head_gain: float32 [512], replicated, may hold values from 0.1 to 1.9
- output_matrix: bfloat16 [1024, 2048], P('tp', 'fs'), may hold values from -2.4375 to 2.4375
- attention_post_gain: float32 [2048], P('tp'), may hold values from 0.1 to 1.9
- feedforward_pre_gain: float32 [2048], replicated, may hold values from 0.1 to 1.9
- up_matrix: bfloat16 [2048, 4096], P('fs', 'tp'), may hold values from -0.125 to 0.125
- down_matrix: bfloat16 [4096, 2048], P('tp', 'fs'), may hold values from -1.21875 to 1.21875
- feedforward_post_gain: float32 [2048], P('tp'), may hold values from 0.1 to 1.9
Outputs:
- layer_out: bfloat16 [16384, 2048], P(('rep', 'fs'), 'tp')
All inputs are finite; a program needn't handle non-finite values.
Results may differ from a plain program's by a relative error of at most 0.017.
Values may be sent and summed in bfloat16 or wider, within the bound.
A program may use at most 128 MiB of HBM per device.

v0:
```python
import jax
import jax.numpy as jnp
from jax import lax
from jax.sharding import PartitionSpec as P

KEY_WIDTH = 256
DV = 512
BLOCK = 64


EPS = 1e-06


def pre_norm(rows, gain):
    values = rows.astype(jnp.float32)
    scale = lax.rsqrt(jnp.mean(values * values, axis=-1, keepdims=True) + EPS)
    return (values * scale * gain).astype(jnp.bfloat16)


def block_attention(queries, keys_in, values_in, log_gates):
    head_count, token_length, key_size = queries.shape
    value_size = values_in.shape[-1]
    blocks = token_length // BLOCK

    def to_blocks(array):
        return array.reshape(head_count, blocks, BLOCK, array.shape[-1]).transpose(1, 0, 2, 3)

    causal = jnp.tril(jnp.ones((BLOCK, BLOCK), dtype=bool))[None, :, :, None]
    highest = lax.Precision.HIGHEST

    def advance(memory_state, inputs):
        query_blk, key_blk, value_blk, gate_blk = inputs
        cumulative = jnp.cumsum(gate_blk, axis=1)
        carried = jnp.einsum(
            "hid,hde->hie", query_blk * jnp.exp(cumulative), memory_state, precision=highest
        )
        spread_log = cumulative[:, :, None, :] - cumulative[:, None, :, :]
        weights = jnp.exp(jnp.where(causal, spread_log, -jnp.inf))
        scores = jnp.einsum("hid,hjd,hijd->hij", query_blk, key_blk, weights, precision=highest)
        readout = carried + jnp.einsum("hij,hje->hie", scores, value_blk, precision=highest)
        final_log = cumulative[:, -1:, :]
        memory_state = jnp.exp(final_log[:, 0, :])[:, :, None] * memory_state + jnp.einsum(
            "hjd,hje->hde", key_blk * jnp.exp(final_log - cumulative), value_blk, precision=highest
        )
        return (memory_state, readout)

    start_state = jnp.zeros((head_count, key_size, value_size), jnp.float32)
    _, readout = lax.scan(
        advance,
        start_state,
        (to_blocks(queries), to_blocks(keys_in), to_blocks(values_in), to_blocks(log_gates)),
    )
    return readout.transpose(1, 0, 2, 3).reshape(head_count, token_length, value_size)


def make_adder(left):

    def add_rows(total, piece, start):
        return jnp.dot(left, piece, preferred_element_type=jnp.float32)

    return add_rows


def make_projector(left, piece):
    return jnp.dot(left, piece, preferred_element_type=jnp.float32)


def on_device(
    tokens,
    attention_pre_gain,
    query_matrix,
    key_matrix,
    value_matrix,
    decay_first_weight,
    decay_second_weight,
    decay_offset_bias,
    extra_log_surge,
    readout_head_gain,
    output_matrix,
    attention_post_gain,
    feedforward_pre_gain,
    up_matrix,
    down_matrix,
    feedforward_post_gain,
):
    token_length = tokens.shape[0]
    gathered = lax.all_gather(tokens, "tp", axis=1, tiled=True)
    width = gathered.shape[1]
    normed = pre_norm(gathered, attention_pre_gain)
    add_rows = make_adder(normed)
    key_cols = query_matrix.shape[1]
    value_cols = value_matrix.shape[1]
    empty_key = jnp.zeros((token_length, key_cols), jnp.float32)
    empty_value = jnp.zeros((token_length, value_cols), jnp.float32)
    start = jnp.int32(0)
    query_proj = add_rows(empty_key, lax.all_gather(query_matrix, "fs", axis=0, tiled=True), start)
    key_proj = add_rows(empty_key, lax.all_gather(key_matrix, "fs", axis=0, tiled=True), start)
    value_proj = add_rows(
        empty_value, lax.all_gather(value_matrix, "fs", axis=0, tiled=True), start
    )
    query_proj = query_proj.astype(jnp.bfloat16)
    key_proj = key_proj.astype(jnp.bfloat16)
    value_proj = value_proj.astype(jnp.bfloat16)
    rank_rows = jnp.dot(normed, decay_first_weight, preferred_element_type=jnp.float32).astype(
        jnp.bfloat16
    )
    gate_source_input = (
        jnp.dot(rank_rows, decay_second_weight, preferred_element_type=jnp.float32)
        + decay_offset_bias
    )
    head_count = key_cols // KEY_WIDTH
    logarithm_decay = (jax.nn.log_sigmoid(gate_source_input) / 16.0).reshape(
        token_length, head_count, KEY_WIDTH
    ) + extra_log_surge[:, :, None]

    def by_head(array, size):
        return array.astype(jnp.float32).reshape(token_length, head_count, size).transpose(1, 0, 2)

    queries = by_head(query_proj, KEY_WIDTH) * KEY_WIDTH ** (-0.5)
    readout = block_attention(
        queries,
        by_head(key_proj, KEY_WIDTH),
        by_head(value_proj, DV),
        logarithm_decay.transpose(1, 0, 2),
    )
    readout = readout.transpose(1, 0, 2)
    head_scale = lax.rsqrt(jnp.mean(readout * readout, axis=-1, keepdims=True) + EPS)
    mixed = (
        (readout * head_scale * readout_head_gain)
        .astype(jnp.bfloat16)
        .reshape(token_length, value_cols)
    )
    partial_attn = make_projector(mixed, lax.all_gather(output_matrix, "fs", axis=1, tiled=True))
    attn = lax.psum_scatter(
        partial_attn.astype(jnp.bfloat16), "tp", scatter_dimension=1, tiled=True
    ).astype(jnp.float32)
    attn_total = lax.psum(jnp.sum(attn * attn, axis=1), "tp")
    attn_scale = lax.rsqrt(attn_total / width + EPS)[:, None]
    resid = (tokens.astype(jnp.float32) + attn * attn_scale * attention_post_gain).astype(
        jnp.bfloat16
    )
    gathered_mid = lax.all_gather(resid, "tp", axis=1, tiled=True)
    normed_mid = pre_norm(gathered_mid, feedforward_pre_gain)
    whole_up = lax.all_gather(up_matrix, "fs", axis=0, tiled=True)
    hidden = jnp.dot(normed_mid, whole_up, preferred_element_type=jnp.float32)
    hidden = jax.nn.relu(hidden)
    squared = (hidden * hidden).astype(jnp.bfloat16)
    partial_feed = make_projector(squared, lax.all_gather(down_matrix, "fs", axis=1, tiled=True))
    feed = lax.psum_scatter(
        partial_feed.astype(jnp.bfloat16), "tp", scatter_dimension=1, tiled=True
    ).astype(jnp.float32)
    feed_total = lax.psum(jnp.sum(feed * feed, axis=1), "tp")
    feed_scale = lax.rsqrt(feed_total / width + EPS)[:, None]
    return (resid.astype(jnp.float32) + feed * feed_scale * feedforward_post_gain).astype(
        jnp.bfloat16
    )


def solution(mesh):
    return jax.shard_map(
        on_device,
        mesh=mesh,
        in_specs=(
            P(("rep", "fs"), "tp"),
            P(),
            P("fs", "tp"),
            P("fs", "tp"),
            P("fs", "tp"),
            P(),
            P(None, "tp"),
            P("tp"),
            P(("rep", "fs"), "tp"),
            P(),
            P("tp", "fs"),
            P("tp"),
            P(),
            P("fs", "tp"),
            P("tp", "fs"),
            P("tp"),
        ),
        out_specs=P(("rep", "fs"), "tp"),
        check_vma=False,
    )
```

profile of v0, /device:TPU:0, one launch (start us, length us, event | category | flops | bytes accessed | tf_op | source)
XLA Modules:
  0.0 660.1 jit_solution(7252431059757820232)
XLA Ops:
  10.0 15.3 %all-gather.9.cloned.1.call-done = bf16[1024,2048]{1,0:T(8,128)(2,1)} async-done(((bf16[1024,1024]{1,0:T(8,128)(2,1)}), bf16[1024,2048]{1,0:T(8,128)(2,1)}) %all-gather.9.cloned.1.call-update) | async-done | bytes 4194320 | tf_op jit(solution)/shard_map/all_gather | solution.py:87
  25.3 3.2 fusion.30
  28.8 3.0 fusion.32
  31.7 46.0 %all-gather.13.cloned.1.call-done = bf16[2048,512]{1,0:T(8,128)(2,1)} async-done(((bf16[256,512]{1,0:T(8,128)(2,1)}), bf16[2048,512]{1,0:T(8,128)(2,1)}) %all-gather.13.cloned.1.call-update) | async-done | bytes 2097168 | tf_op jit(solution)/shard_map/all_gather | solution.py:99
  77.7 5.2 convolution_convert_fusion.1
  84.5 34.2 %all-gather.11.cloned.1.call-done = bf16[2048,256]{1,0:T(8,128)(2,1)} async-done(((bf16[256,256]{1,0:T(8,128)(2,1)}), bf16[2048,256]{1,0:T(8,128)(2,1)}) %all-gather.11.cloned.1.call-update) | async-done | bytes 1048592 | tf_op jit(solution)/shard_map/all_gather | solution.py:97
  118.7 3.7 convolution_convert_fusion.3
  123.6 5.1 fusion.63
  128.7 31.0 %all-gather.15.cloned.1.call-done = bf16[2048,256]{1,0:T(8,128)(2,1)} async-done(((bf16[256,256]{1,0:T(8,128)(2,1)}), bf16[2048,256]{1,0:T(8,128)(2,1)}) %all-gather.15.cloned.1.call-update) | async-done | bytes 1048592 | tf_op jit(solution)/shard_map/all_gather | solution.py:96
  159.7 4.8 fusion.60
  164.5 150.9 %while.13 = (s32[]{:T(128)}, f32[1,256,512]{2,1,0:T(8,128)S(1)}, f32[16,1,64,512]{3,2,1,0:T(8,128)S(1)}, f32[16,1,64,256]{3,2,1,0:T(8,128)}, f32[16,1,64,256]{3,...) while((s32[]{:T(128)}, f32[1,256,512]{2,1,0:T(8,128)S(1)}, ...), condition=%wide.region_3.4_spmd.clone, body=%wide.region_1.3_spmd.clone.sunk | while | flops 233373696 | bytes 11649660 | solution.py:48
  167.2 2.5 fusion.98
  176.6 2.5 fusion.98
  186.1 2.5 fusion.98
  195.5 2.5 fusion.98
  204.9 2.5 fusion.98
  214.4 2.5 fusion.98
  223.8 2.5 fusion.98
  233.2 2.5 fusion.98
  242.7 2.5 fusion.98
  252.1 2.5 fusion.98
  261.5 2.5 fusion.98
  316.0 5.9 convolution_convert_fusion
  322.0 10.7 %reduce-scatter.3.cloned.1.call-done = bf16[1024,1024]{1,0:T(8,128)(2,1)} async-done(((bf16[1024,2048]{1,0:T(8,128)(2,1)}), bf16[1024,1024]{1,0:T(8,128)(2,1)}) %reduce-scatter.3.cloned.1.call-update) | async-done | bytes 2097168 | tf_op jit(solution)/shard_map/reduce_scatter | solution.py:134
  337.2 3.7 fusion.39
  342.5 13.6 %all-gather.19.cloned.1.call-done = bf16[1024,2048]{1,0:T(8,128)(2,1)} async-done(((bf16[1024,1024]{1,0:T(8,128)(2,1)}), bf16[1024,2048]{1,0:T(8,128)(2,1)}) %all-gather.19.cloned.1.call-update) | async-done | bytes 4194320 | tf_op jit(solution)/shard_map/all_gather | solution.py:142
  356.1 3.1 fusion.33
  359.2 124.7 %all-gather.21.cloned.1.call-done = bf16[2048,2048]{1,0:T(8,128)(2,1)} async-done(((bf16[256,2048]{1,0:T(8,128)(2,1)}), bf16[2048,2048]{1,0:T(8,128)(2,1)}) %all-gather.21.cloned.1.call-update) | async-done | bytes 8388624 | tf_op jit(solution)/shard_map/all_gather | solution.py:144
  483.9 125.2 %all-gather.23.cloned.1.call-done = bf16[2048,2048]{1,0:T(8,128)(2,1)} async-done(((bf16[2048,256]{1,0:T(8,128)(2,1)}), bf16[2048,2048]{1,0:T(8,128)(2,1)}) %all-gather.23.cloned.1.call-update) | async-done | bytes 8388624 | tf_op jit(solution)/shard_map/all_gather | solution.py:148
  609.1 25.6 %fusion.53 = bf16[1024,2048]{1,0:T(8,128)(2,1)} fusion(bf16[2048,2048]{1,0:T(8,128)(2,1)} %all-gather.23.cloned.1.call-done, bf16[2048,2048]{1,0:T(8,128)(2,1)} %all-gather.21.cloned.1.call-done, bf16[1024,2048]{1,0:T(8,128)(2,1)} %all-gather.19.cloned.1.call-done, f32[2048]{0:T(1024)S(1)} %copy-done.10, f32[1024]{0:T(1024)S(1)} %add_rsqrt_fusion.2), kind=kOutput, calls=%fused_computation.65 | convolution fusion | flops 17196646400 | bytes 25178112 | tf_op jit(solution)/shard_map/dot_general | solution.py:65
  634.7 10.2 %reduce-scatter.5.cloned.1.call-done = bf16[1024,1024]{1,0:T(8,128)(2,1)} async-done(((bf16[1024,2048]{1,0:T(8,128)(2,1)}), bf16[1024,1024]{1,0:T(8,128)(2,1)}) %reduce-scatter.5.cloned.1.call-update) | async-done | bytes 2097168 | tf_op jit(solution)/shard_map/reduce_scatter | solution.py:149
  649.5 3.7 fusion.43
  (228 shorter events, 139.8 us)
Async XLA Ops:
  6.5 117.0 %copy-start = (bf16[2048,16]{0,1:T(8,128)(2,1)S(1)}, bf16[2048,16]{0,1:T(8,128)(2,1)}, u32[]{:S(2)}) copy-start(bf16[2048,16]{0,1:T(8,128)(2,1)} %param.23) | copy-start | bytes 196612
  6.5 22.0 %copy-start.5 = (f32[2048]{0:T(1024)S(1)}, f32[2048]{0:T(1024)}, u32[]{:S(2)}) copy-start(f32[2048]{0:T(1024)} %param.19) | copy-start | bytes 24580
  6.5 18.8 %all-gather.9.cloned.1.call-start = ((), (), s32[]{:S(2)}) async-start(), calls=%async_computation.2 | async-start | bytes 6291456 | tf_op jit(solution)/shard_map/all_gather | solution.py:87
  7.3 70.5 %all-gather.13.cloned.1.call-start = ((), (), s32[]{:S(2)}) async-start(), calls=%async_computation.4 | async-start | bytes 2359296 | tf_op jit(solution)/shard_map/all_gather | solution.py:99
  8.0 110.7 %all-gather.11.cloned.1.call-start = ((), (), s32[]{:S(2)}) async-start(), calls=%async_computation.3 | async-start | bytes 1179648 | tf_op jit(solution)/shard_map/all_gather | solution.py:97
  8.7 151.0 %all-gather.15.cloned.1.call-start = ((), (), s32[]{:S(2)}) async-start(), calls=%async_computation.5 | async-start | bytes 1179648 | tf_op jit(solution)/shard_map/all_gather | solution.py:96
  9.3 306.7 %all-gather.17.cloned.1.call-start = ((), (), s32[]{:S(2)}) async-start(), calls=%async_computation.6 | async-start | bytes 2359296 | tf_op jit(solution)/shard_map/all_gather | solution.py:133
  9.9 322.7 %reduce-scatter.3.cloned.1.call-start = ((), (), s32[]{:S(2)}) async-start(), calls=%async_computation.7 | async-start | bytes 6291456 | tf_op jit(solution)/shard_map/reduce_scatter | solution.py:134
  25.3 3.4 copy-start.3
  84.5 39.0 %copy-start.9 = (bf16[16,256]{1,0:T(8,128)(2,1)S(1)}, bf16[16,256]{1,0:T(8,128)(2,1)}, u32[]{:S(2)}) copy-start(bf16[16,256]{1,0:T(8,128)(2,1)} %param.24) | copy-start | bytes 24580
  84.5 39.0 %copy-start.11 = (f32[1024,1]{0,1:T(1,128)S(1)}, f32[1024,1]{0,1:T(1,128)}, u32[]{:S(2)}) copy-start(f32[1024,1]{0,1:T(1,128)} %param.26) | copy-start | bytes 12292
  84.5 39.0 %copy-start.12 = (f32[256]{0:T(256)S(1)}, f32[256]{0:T(256)}, u32[]{:S(2)}) copy-start(f32[256]{0:T(256)} %param.25) | copy-start | bytes 3076
  164.5 151.2 %copy-start.8 = (f32[512]{0:T(512)S(1)}, f32[512]{0:T(512)}, u32[]{:S(2)}) copy-start(f32[512]{0:T(512)} %param.27) | copy-start | bytes 6148
  321.9 15.3 %copy-start.4 = (bf16[1024,1024]{1,0:T(8,128)(2,1)S(1)}, bf16[1024,1024]{1,0:T(8,128)(2,1)}, u32[]{:S(2)}) copy-start(bf16[1024,1024]{1,0:T(8,128)(2,1)} %param.18) | copy-start | bytes 6291460
  321.9 15.3 %copy-start.6 = (f32[1024]{0:T(1024)S(1)}, f32[1024]{0:T(1024)}, u32[]{:S(2)}) copy-start(f32[1024]{0:T(1024)} %param.29) | copy-start | bytes 12292
  321.9 34.2 %all-gather.19.cloned.1.call-start = ((), (), s32[]{:S(2)}) async-start(), calls=%async_computation.8 | async-start | bytes 6291456 | tf_op jit(solution)/shard_map/all_gather | solution.py:142
  340.9 268.2 %copy-start.10 = (f32[2048]{0:T(1024)S(1)}, f32[2048]{0:T(1024)}, u32[]{:S(2)}) copy-start(f32[2048]{0:T(1024)} %param.30) | copy-start | bytes 24580
  341.0 142.9 %all-gather.21.cloned.1.call-start = ((), (), s32[]{:S(2)}) async-start(), calls=%async_computation.9 | async-start | bytes 9437184 | tf_op jit(solution)/shard_map/all_gather | solution.py:144
  341.7 267.4 %all-gather.23.cloned.1.call-start = ((), (), s32[]{:S(2)}) async-start(), calls=%async_computation.10 | async-start | bytes 9437184 | tf_op jit(solution)/shard_map/all_gather | solution.py:148
  342.4 302.5 %reduce-scatter.5.cloned.1.call-start = ((), (), s32[]{:S(2)}) async-start(), calls=%async_computation.11 | async-start | bytes 6291456 | tf_op jit(solution)/shard_map/reduce_scatter | solution.py:149
  634.7 14.8 %copy-start.2 = (bf16[1024,1024]{1,0:T(8,128)(2,1)S(1)}, bf16[1024,1024]{1,0:T(8,128)(2,1)}, u32[]{:S(2)}) copy-start(bf16[1024,1024]{1,0:T(8,128)(2,1)} %fusion.39) | copy-start | bytes 6291460
  634.7 14.8 %copy-start.7 = (f32[1024]{0:T(1024)S(1)}, f32[1024]{0:T(1024)}, u32[]{:S(2)}) copy-start(f32[1024]{0:T(1024)} %param.33) | copy-start | bytes 12292
  634.7 18.5 %copy-start.1 = (bf16[2048,16]{0,1:T(8,128)(2,1)S(1)}, bf16[2048,16]{0,1:T(8,128)(2,1)}, u32[]{:S(2)}) copy-start(bf16[2048,16]{0,1:T(8,128)(2,1)} %param.23) | copy-start | bytes 196612
Sparse Core Ops, SparseCore 0:
  8.9 16.3 all-gather.8
  27.4 50.2 all-gather.12
  79.8 38.7 all-gather.10
  120.7 38.9 all-gather.14
  161.6 49.1 all-gather.16
  322.0 10.5 reduce-scatter.2
  341.1 14.9 all-gather.18
  358.2 125.6 all-gather.20
  485.9 123.1 all-gather.22
  634.9 10.0 reduce-scatter.4
where the time goes:
time: 663 us; the launch traced here: 660 us
  waiting for transfers between devices  415 us (63%)
  matrix products  117 us (18%)
  other arithmetic  79.4 us (12%)
  local copies, waits for them, and re-layouts  28.2 us (4%)
  between operations  13.7 us (2%)
    all_gather x1, waiting for transfers between devices, on_device(): lax.all_gather(down_matrix, 'fs', axis=1, tiled=True)  125 us
    all_gather x1, waiting for transfers between devices, on_device(): whole_up = lax.all_gather(up_matrix, 'fs', axis=0, tiled=True)  125 us
    all_gather x1, waiting for transfers between devices, on_device(): lax.all_gather(value_matrix, 'fs', axis=0, tiled=True)  46 us
    dot_general x16, other arithmetic, advance(): jnp.einsum('hid,hjd,hijd->hij', query_blk, key_blk, weights, precision=hi...  40.2 us
    all_gather x1, waiting for transfers between devices, on_device(): lax.all_gather(key_matrix, 'fs', axis=0, tiled=True)  34.2 us
    dot_general x2, matrix products, make_projector(): return jnp.dot(left, piece, preferred_element_type=jnp.float32)  31.5 us
    all_gather x1, waiting for transfers between devices, on_device(): lax.all_gather(query_matrix, 'fs', axis=0, tiled=True)  31 us
    dot_general x16, matrix products, advance(): jnp.einsum('hjd,hje->hde', key_blk * jnp.exp(final_log - cumulative), val...  26.3 us
  transfers between devices with their start and end apart: 10, of which 9 were waited for; matrix products, arithmetic and copies ran while one was open for 27% of the time, Pallas kernels for 0%

commit v1 on v0

v1 whole, which is shorter than its diff:
```python
import functools

import jax
import jax.numpy as jnp
from jax import lax
from jax.experimental import pallas as pl
from jax.experimental.pallas import tpu as pltpu
from jax.sharding import PartitionSpec as P

KEY_WIDTH = 256
DV = 512
LENGTH = 1024
CHUNK = 128
SUB = 16
EPS = 1e-06


def pre_norm(rows, gain):
    values = rows.astype(jnp.float32)
    scale = lax.rsqrt(jnp.mean(values * values, axis=-1, keepdims=True) + EPS)
    return (values * scale * gain).astype(jnp.bfloat16)


def attention_kernel(
    q_ref, k_ref, v_ref, rank_ref, second_ref, bias_ref, surge_ref, gain_ref, o_ref, state
):
    subs = CHUNK // SUB

    @pl.when(lax.rem(pl.program_id(1), LENGTH // CHUNK) == 0)
    def _():
        state[...] = jnp.zeros_like(state)

    q = q_ref[...].astype(jnp.float32) * KEY_WIDTH ** (-0.5)
    k = k_ref[...].astype(jnp.float32)
    v = v_ref[...]
    source = (
        jnp.dot(rank_ref[...], second_ref[...], preferred_element_type=jnp.float32)
        + bias_ref[...]
    )
    log_sig = jnp.minimum(source, 0.0) - jnp.log1p(jnp.exp(-jnp.abs(source)))
    gate = log_sig / 16.0 + surge_ref[0]

    row = lax.broadcasted_iota(jnp.int32, (CHUNK, CHUNK), 0)
    col = lax.broadcasted_iota(jnp.int32, (CHUNK, CHUNK), 1)
    lower = (row >= col).astype(jnp.float32)
    cum = jnp.dot(
        lower, gate, preferred_element_type=jnp.float32, precision=lax.Precision.HIGHEST
    )

    q3 = q.reshape(subs, SUB, KEY_WIDTH)
    k3 = k.reshape(subs, SUB, KEY_WIDTH)
    c3 = cum.reshape(subs, SUB, KEY_WIDTH)
    pick_col = lax.rem(lax.broadcasted_iota(jnp.int32, (KEY_WIDTH, CHUNK), 1), SUB)
    scores = jnp.zeros((CHUNK, CHUNK), jnp.float32)
    for j in range(SUB):
        weight = jnp.exp(jnp.minimum(c3 - c3[:, j : j + 1, :], 0.0))
        term = (q3 * k3[:, j : j + 1, :] * weight).reshape(CHUNK, KEY_WIDTH)
        scores += jnp.dot(
            term.astype(jnp.bfloat16),
            (pick_col == j).astype(jnp.bfloat16),
            preferred_element_type=jnp.float32,
        )
    scores = jnp.where((row // SUB == col // SUB) & (row >= col), scores, 0.0)

    pieces = [jnp.zeros((SUB, CHUNK), jnp.float32)]
    key_row = lax.broadcasted_iota(jnp.int32, (CHUNK, KEY_WIDTH), 0)
    for i in range(1, subs):
        edge = cum[i * SUB - 1 : i * SUB, :]
        left = q3[i] * jnp.exp(jnp.minimum(c3[i] - edge, 0.0))
        right = jnp.where(key_row < i * SUB, k * jnp.exp(jnp.minimum(edge - cum, 0.0)), 0.0)
        pieces.append(
            lax.dot_general(
                left.astype(jnp.bfloat16),
                right.astype(jnp.bfloat16),
                (((1,), (1,)), ((), ())),
                preferred_element_type=jnp.float32,
            )
        )
    scores = scores + jnp.concatenate(pieces, axis=0)

    last = cum[CHUNK - 1 : CHUNK, :]
    held = state[...]
    readout = lax.dot_general(
        (q * jnp.exp(cum)).astype(jnp.bfloat16),
        held.astype(jnp.bfloat16),
        (((1,), (1,)), ((), ())),
        preferred_element_type=jnp.float32,
    ) + jnp.dot(scores.astype(jnp.bfloat16), v, preferred_element_type=jnp.float32)
    faded = (k * jnp.exp(jnp.minimum(last - cum, 0.0))).astype(jnp.bfloat16)
    state[...] = held * jnp.exp(last) + lax.dot_general(
        v, faded, (((0,), (0,)), ((), ())), preferred_element_type=jnp.float32
    )
    scale = lax.rsqrt(jnp.mean(readout * readout, axis=-1, keepdims=True) + EPS)
    o_ref[...] = (readout * scale * gain_ref[...]).astype(jnp.bfloat16)


def attention(qkv, rank_rows, second, bias, surge, gain):
    tokens = qkv.shape[0]
    heads = second.shape[1] // KEY_WIDTH
    rank = rank_rows.shape[1]
    value_base = 2 * heads * KEY_WIDTH // DV
    return pl.pallas_call(
        attention_kernel,
        grid=(heads, tokens // CHUNK),
        in_specs=[
            pl.BlockSpec((CHUNK, KEY_WIDTH), lambda h, c: (c, h)),
            pl.BlockSpec((CHUNK, KEY_WIDTH), lambda h, c: (c, heads + h)),
            pl.BlockSpec((CHUNK, DV), lambda h, c: (c, value_base + h)),
            pl.BlockSpec((CHUNK, rank), lambda h, c: (c, 0)),
            pl.BlockSpec((rank, KEY_WIDTH), lambda h, c: (0, h)),
            pl.BlockSpec((1, KEY_WIDTH), lambda h, c: (0, h)),
            pl.BlockSpec((1, CHUNK, 1), lambda h, c: (h, c, 0)),
            pl.BlockSpec((1, DV), lambda h, c: (0, 0)),
        ],
        out_specs=pl.BlockSpec((CHUNK, DV), lambda h, c: (c, h)),
        out_shape=jax.ShapeDtypeStruct((tokens, heads * DV), jnp.bfloat16),
        scratch_shapes=[pltpu.VMEM((DV, KEY_WIDTH), jnp.float32)],
        compiler_params=pltpu.CompilerParams(
            dimension_semantics=("arbitrary", "arbitrary"), vmem_limit_bytes=24 * 2**20
        ),
        cost_estimate=pl.CostEstimate(
            flops=20_000_000_000, bytes_accessed=20_000_000, transcendentals=8_000_000
        ),
        name="attention",
    )(qkv, qkv, qkv, rank_rows, second, bias[None, :], surge.T[:, :, None], gain[None, :])


def on_device(
    n_rep,
    n_tp,
    tokens,
    attention_pre_gain,
    query_matrix,
    key_matrix,
    value_matrix,
    decay_first_weight,
    decay_second_weight,
    decay_offset_bias,
    extra_log_surge,
    readout_head_gain,
    output_matrix,
    attention_post_gain,
    feedforward_pre_gain,
    up_matrix,
    down_matrix,
    feedforward_post_gain,
):
    me = lax.axis_index("tp")
    rep = lax.axis_index("rep")
    swap = [(i, 1 - i) for i in range(2)]

    def both_halves(mine):
        if n_tp != 2:
            return lax.all_gather(mine, "tp", axis=1, tiled=True)
        other = lax.ppermute(mine, "tp", swap)
        first = me == 0
        return jnp.concatenate(
            [jnp.where(first, mine, other), jnp.where(first, other, mine)], axis=1
        )

    def sum_scattered(partial):
        if n_tp != 2:
            return lax.psum_scatter(partial, "tp", scatter_dimension=1, tiled=True).astype(
                jnp.float32
            )
        size = partial.shape[1] // 2
        keep = lax.dynamic_slice_in_dim(partial, me * size, size, 1)
        send = lax.dynamic_slice_in_dim(partial, (1 - me) * size, size, 1)
        return keep.astype(jnp.float32) + lax.ppermute(send, "tp", swap).astype(jnp.float32)

    def summed(rows):
        if n_tp != 2:
            return lax.psum(rows, "tp")
        return rows + lax.ppermute(rows, "tp", swap)

    def part(weight, axis):
        size = weight.shape[axis] // n_rep
        return lax.dynamic_slice_in_dim(weight, rep * size, size, axis)

    weights = jnp.concatenate([query_matrix, key_matrix, value_matrix], axis=1)
    with jax.named_scope("gather_in"):
        whole_in = lax.all_gather(weights, "fs", axis=0, tiled=True)
    with jax.named_scope("gather_out"):
        whole_out = lax.all_gather(output_matrix, "fs", axis=1, tiled=True)
    with jax.named_scope("gather_up"):
        whole_up = lax.all_gather(part(up_matrix, 1), ("rep", "fs"), axis=0, tiled=True)
    with jax.named_scope("gather_down"):
        whole_down = lax.all_gather(part(down_matrix, 0), ("rep", "fs"), axis=1, tiled=True)

    gathered = both_halves(tokens)
    width = gathered.shape[1]
    normed = pre_norm(gathered, attention_pre_gain)
    rank_rows = jnp.dot(normed, decay_first_weight, preferred_element_type=jnp.float32).astype(
        jnp.bfloat16
    )
    with jax.named_scope("project"):
        qkv = jnp.dot(normed, whole_in, preferred_element_type=jnp.float32).astype(jnp.bfloat16)
    with jax.named_scope("mix"):
        mixed = attention(
            qkv, rank_rows, decay_second_weight, decay_offset_bias, extra_log_surge,
            readout_head_gain,
        )
    with jax.named_scope("out_project"):
        partial_attn = jnp.dot(mixed, whole_out, preferred_element_type=jnp.float32)
    attn = sum_scattered(partial_attn.astype(jnp.bfloat16))
    attn_total = summed(jnp.sum(attn * attn, axis=1))
    attn_scale = lax.rsqrt(attn_total / width + EPS)[:, None]
    resid = (tokens.astype(jnp.float32) + attn * attn_scale * attention_post_gain).astype(
        jnp.bfloat16
    )
    normed_mid = pre_norm(both_halves(resid), feedforward_pre_gain)
    up_parts = whole_up.reshape(n_rep, width, -1)
    squared = []
    for r in range(n_rep):
        hidden = jax.nn.relu(
            jnp.dot(normed_mid, up_parts[r], preferred_element_type=jnp.float32)
        )
        squared.append((hidden * hidden).astype(jnp.bfloat16))
    partial_feed = sum(
        jnp.dot(
            squared[r],
            whole_down[:, r * width : (r + 1) * width],
            preferred_element_type=jnp.float32,
        )
        for r in range(n_rep)
    )
    feed = sum_scattered(partial_feed.astype(jnp.bfloat16))
    feed_total = summed(jnp.sum(feed * feed, axis=1))
    feed_scale = lax.rsqrt(feed_total / width + EPS)[:, None]
    return (resid.astype(jnp.float32) + feed * feed_scale * feedforward_post_gain).astype(
        jnp.bfloat16
    )


def solution(mesh):
    return jax.shard_map(
        functools.partial(on_device, mesh.shape["rep"], mesh.shape["tp"]),
        mesh=mesh,
        in_specs=(
            P(("rep", "fs"), "tp"),
            P(),
            P("fs", "tp"),
            P("fs", "tp"),
            P("fs", "tp"),
            P(),
            P(None, "tp"),
            P("tp"),
            P(("rep", "fs"), "tp"),
            P(),
            P("tp", "fs"),
            P("tp"),
            P(),
            P("fs", "tp"),
            P("tp", "fs"),
            P("tp"),
        ),
        out_specs=P(("rep", "fs"), "tp"),
        check_vma=False,
    )
```

time: 663 us -> 418 us (0.63)
  waiting for transfers between devices: 415 us -> 314 us
  matrix products: 117 us -> 48.3 us
  other arithmetic: 79.4 us -> 18.5 us
  local copies, waits for them, and re-layouts: 28.2 us -> 9.15 us
  Pallas kernels: 0 us -> 13.2 us
    all_gather x8 -> x4, waiting for transfers between devices: 390 us -> 295 us  [the longest x1 118 us: on_device(): lax.all_gather(part(down_matrix, 0), ('rep', 'fs'), axis=1, tiled=True)]
    dot_general x54 -> x7, matrix products: 117 us -> 48.3 us  [the longest x2 17.6 us: on_device(): jnp.dot(squared[r], whole_down[:, r * width:(r + 1) * width], preferred_e...]
    dot_general x16 -> x0, other arithmetic: 40.2 us -> none  [advance(): jnp.einsum('hid,hjd,hijd->hij', query_blk, key_blk, weights, precision=hi...]
    reduce_scatter x2 -> x0, waiting for transfers between devices: 20.9 us -> none  [the longest x1 10.7 us: on_device(): lax.psum_scatter(partial_attn.astype(jnp.bfloat16), 'tp', scatter_dimensi...]
    ppermute x0 -> x6, waiting for transfers between devices: none -> 18.3 us  [the longest x2 8.51 us: sum_scattered(): lax.ppermute(send, 'tp', swap).astype(jnp.float32)]
    another operation x16 -> x0, local copies, waits for them, and re-layouts: 14.2 us -> none
    squeeze x16 -> x0, local copies, waits for them, and re-layouts: 13.6 us -> none  [block_attention(): lax.scan(advance, start_state, (to_blocks(queries), to_blocks(keys_in), t...]
    exp x16 -> x0, other arithmetic: 13.4 us -> none  [advance(): weights = jnp.exp(jnp.where(causal, spread_log, -jnp.inf))]
  transfers between devices with their start and end apart: 10 -> 10, of which waited for: 9 -> 10; matrix products, arithmetic and copies ran while one was open for 27% -> 12% of each run, Pallas kernels for 0% -> 3%
where the time goes in v1:
time: 418 us
  waiting for transfers between devices  314 us (75%)
  matrix products  48.3 us (12%)
  other arithmetic  18.5 us (4%)
  between operations  13.4 us (3%)
  Pallas kernels  13.2 us (3%)
  local copies, waits for them, and re-layouts  9.15 us (2%)
    all_gather x1, waiting for transfers between devices, on_device(): lax.all_gather(part(down_matrix, 0), ('rep', 'fs'), axis=1, tiled=True)  118 us
    all_gather x1, waiting for transfers between devices, on_device(): lax.all_gather(part(up_matrix, 1), ('rep', 'fs'), axis=0, tiled=True)  84.2 us
    all_gather x1, waiting for transfers between devices, on_device(): whole_in = lax.all_gather(weights, 'fs', axis=0, tiled=True)  62.5 us
    all_gather x1, waiting for transfers between devices, on_device(): whole_out = lax.all_gather(output_matrix, 'fs', axis=1, tiled=True)  29.7 us
    dot_general x2, matrix products, on_device(): jnp.dot(squared[r], whole_down[:, r * width:(r + 1) * width], preferred_e...  17.6 us
    dot_general x2, matrix products, on_device(): jnp.dot(normed_mid, up_parts[r], preferred_element_type=jnp.float32)  17.1 us
    pallas_call x1, Pallas kernels, attention(): pl.pallas_call(attention_kernel, grid=(heads, tokens // CHUNK), in_specs=...  13.2 us
    ppermute x2, waiting for transfers between devices, sum_scattered(): lax.ppermute(send, 'tp', swap).astype(jnp.float32)  8.51 us
  transfers between devices with their start and end apart: 10, of which 10 were waited for; matrix products, arithmetic and copies ran while one was open for 12% of the time, Pallas kernels for 3%

profile of v1, /device:TPU:0, one launch (start us, length us, event | category | flops | bytes accessed | tf_op | source)
XLA Modules:
  0.0 417.6 jit_solution(864556190943422250)
XLA Ops:
  6.5 2.0 pad_maximum_fusion.2
  9.4 0.8 constant_dynamic-slice_fusion.2
  10.4 2.0 constant_dynamic-slice_fusion.1
  13.1 3.7 collective-permute-done
  16.8 1.9 broadcast_select_fusion.3
  18.7 1.0 fusion
  20.7 1.7 convolution_convert_fusion.2.rank_ref
  22.5 62.5 %all-gather.5.cloned.1.call-done = bf16[2048,1024]{1,0:T(8,128)(2,1)} async-done(((bf16[256,1024]{1,0:T(8,128)(2,1)}), bf16[2048,1024]{1,0:T(8,128)(2,1)}) %all-gather.5.cloned.1.call-update) | async-done | bytes 4194320 | tf_op jit(solution)/shard_map/gather_in/all_gather | solution.py:182
  85.0 8.0 %convolution_convert_fusion.1.q_ref.k_ref.v_ref = bf16[1024,1024]{1,0:T(8,128)(2,1)S(1)} fusion(bf16[2048,1024]{1,0:T(8,128)(2,1)} %all-gather.5.cloned.1.call-done, f32[2048]{0:T(1024)S(1)} %copy-done.19, f32[1024]{0:T(1024)S(1)} %add_rsqrt_fusion.3, bf16[1024,1024]{1,0:T(8,128)(2,1)} %copy-done.12, bf16[1024,1024]{1,0:T(8,128)(2,1)} %copy-done.11), kind=kOutput, calls=%fused_computation.34 | convolution fusion | flops 4310695936 | bytes 10498048 | tf_op jit(solution)/shard_map/project/dot_general | solution.py:197
  93.0 13.2 %attention.1 = bf16[1024,512]{1,0:T(8,128)(2,1)S(1)} custom-call(bf16[1024,1024]{1,0:T(8,128)(2,1)S(1)} %convolution_convert_fusion.1.q_ref.k_ref.v_ref, bf16[1024,1024]{1,0:T(8,128)(2,1)S(1)} %convolution_convert_fusion.1.q_ref.k_ref.v_ref, bf16[1024,1024]{1,0:T(8,128)(2,1)S(1)} %convolution_convert_fusion.1.q_ref.k_ref.v_ref, ...), custom_call_target="tpu_custom_call" | custom-call | flops 20000000000 | bytes 20000000 | tf_op jit(solution)/shard_map/mix/attention/pallas_call | solution.py:102
  106.3 29.7 %all-gather.7.cloned.1.call-done = bf16[512,2048]{1,0:T(8,128)(2,1)} async-done(((bf16[512,256]{1,0:T(8,128)(2,1)}), bf16[512,2048]{1,0:T(8,128)(2,1)}) %all-gather.7.cloned.1.call-update) | async-done | bytes 2097168 | tf_op jit(solution)/shard_map/gather_out/all_gather | solution.py:184
  136.0 3.9 convolution_convert_fusion
  139.9 1.9 copy-done.5
  141.9 1.6 constant_dynamic-slice_fusion.3
  143.4 4.4 %collective-permute-done.1 = bf16[1024,1024]{1,0:T(8,128)(2,1)S(1)} collective-permute-done((bf16[1024,1024]{1,0:T(8,128)(2,1)}, bf16[1024,1024]{1,0:T(8,128)(2,1)S(1)}, u32[]{:S(2)}, u32[]{:S(2)}) %collective-permute-start.1) | collective-permute-done | bytes 2097184 | tf_op jit(solution)/shard_map/ppermute | solution.py:169
  147.8 3.1 multiply_reduce_fusion.1
  151.1 1.0 collective-permute-done.2
  152.2 3.4 add_convert_fusion.2
  155.7 4.0 collective-permute-done.3
  159.7 1.6 broadcast_select_fusion.1
  161.3 1.3 copy-done.9
  162.6 2.4 fusion.3
  165.0 84.2 %all-gather.9.cloned.1.call-done = bf16[4096,1024]{1,0:T(8,128)(2,1)} async-done(((bf16[256,1024]{1,0:T(8,128)(2,1)}), bf16[4096,1024]{1,0:T(8,128)(2,1)}) %all-gather.9.cloned.1.call-update) | async-done | bytes 8388624 | tf_op jit(solution)/shard_map/gather_up/all_gather | solution.py:186
  249.3 9.5 %multiply_convert_fusion.1 = bf16[1024,1024]{1,0:T(8,128)(2,1)} fusion(bf16[4096,1024]{1,0:T(8,128)(2,1)} %all-gather.9.cloned.1.call-done, f32[2048]{0:T(1024)S(1)} %copy-done.20, f32[1024]{0:T(1024)S(1)} %add_rsqrt_fusion.1, bf16[1024,1024]{1,0:T(8,128)(2,1)} %copy-done.9, bf16[1024,1024]{1,0:T(8,128)(2,1)} %get-tuple-element.5), kind=kOutput, calls=%fused_computation.25 | convolution fusion | flops 4312793088 | bytes 10498048 | tf_op jit(solution)/shard_map/dot_general | solution.py:216
  258.8 7.6 %multiply_convert_fusion = bf16[1024,1024]{1,0:T(8,128)(2,1)} fusion(bf16[4096,1024]{1,0:T(8,128)(2,1)S(1)} %copy-done.16, f32[2048]{0:T(1024)S(1)} %copy-done.20, f32[1024]{0:T(1024)S(1)} %add_rsqrt_fusion.1, bf16[1024,1024]{1,0:T(8,128)(2,1)S(1)} %copy-done.10, bf16[1024,1024]{1,0:T(8,128)(2,1)} %get-tuple-element.5), kind=kOutput, calls=%fused_computation.24 | convolution fusion | flops 4312793088 | bytes 10498048 | tf_op jit(solution)/shard_map/dot_general | solution.py:216
  266.4 118.2 %all-gather.11.cloned.1.call-done = bf16[1024,4096]{1,0:T(8,128)(2,1)} async-done(((bf16[1024,256]{1,0:T(8,128)(2,1)}), bf16[1024,4096]{1,0:T(8,128)(2,1)}) %all-gather.11.cloned.1.call-update) | async-done | bytes 8388624 | tf_op jit(solution)/shard_map/gather_down/all_gather | solution.py:188
  384.5 10.7 %fusion.6 = f32[1024,2048]{1,0:T(8,128)} fusion(bf16[1024,1024]{1,0:T(8,128)(2,1)} %multiply_convert_fusion, bf16[1024,4096]{1,0:T(8,128)(2,1)} %all-gather.11.cloned.1.call-done), kind=kOutput, calls=%fused_computation.11 | convolution fusion | flops 4294967296 | bytes 14680064 | tf_op jit(solution)/shard_map/dot_general | solution.py:220
  395.2 6.9 %add_convert_fusion = bf16[1024,2048]{1,0:T(8,128)(2,1)S(1)} fusion(f32[1024,2048]{1,0:T(8,128)} %fusion.6, bf16[1024,1024]{1,0:T(8,128)(2,1)S(1)} %copy-done.21, bf16[1024,4096]{1,0:T(8,128)(2,1)S(1)} %copy-done.17), kind=kOutput, calls=%fused_computation.10 | convolution fusion | flops 4299161600 | bytes 18874368 | tf_op jit(solution)/shard_map/dot_general | solution.py:220
  402.5 4.1 collective-permute-done.4
  406.6 0.7 multiply_reduce_fusion
  407.6 1.0 collective-permute-done.5
  408.6 2.4 add_convert_fusion.1
  (62 shorter events, 3.7 us)
Async XLA Ops:
  6.5 2.9 copy-start
  6.5 5.8 %copy-start.8 = (bf16[1024,1024]{1,0:T(8,128)(2,1)S(1)}, bf16[1024,1024]{1,0:T(8,128)(2,1)}, u32[]{:S(2)}) copy-start(bf16[1024,1024]{1,0:T(8,128)(2,1)} %param.16) | copy-start | bytes 6291460
  6.5 6.4 %copy-start.15 = (f32[1024,1]{0,1:T(1,128)S(1)}, f32[1024,1]{0,1:T(1,128)}, u32[]{:S(2)}) copy-start(f32[1024,1]{0,1:T(1,128)} %param.24) | copy-start | bytes 12292
  6.5 78.5 %all-gather.5.cloned.1.call-start = ((), (), s32[]{:S(2)}) async-start(), calls=%async_computation | async-start | bytes 4718592 | tf_op jit(solution)/shard_map/gather_in/all_gather | solution.py:182
  8.6 127.3 %all-gather.7.cloned.1.call-start = ((), (), s32[]{:S(2)}) async-start(), calls=%async_computation.1 | async-start | bytes 2359296 | tf_op jit(solution)/shard_map/gather_out/all_gather | solution.py:184
  9.4 239.9 %all-gather.9.cloned.1.call-start = ((), (), s32[]{:S(2)}) async-start(), calls=%async_computation.2 | async-start | bytes 8912896 | tf_op jit(solution)/shard_map/gather_up/all_gather | solution.py:186
  10.3 374.2 %all-gather.11.cloned.1.call-start = ((), (), s32[]{:S(2)}) async-start(), calls=%async_computation.3 | async-start | bytes 8912896 | tf_op jit(solution)/shard_map/gather_down/all_gather | solution.py:188
  12.4 4.5 %collective-permute-start = (bf16[1024,1024]{1,0:T(8,128)(2,1)S(1)}, bf16[1024,1024]{1,0:T(8,128)(2,1)}, u32[]{:S(2)}, u32[]{:S(2)}) collective-permute-start(bf16[1024,1024]{1,0:T(8,128)(2,1)S(1)} %copy-done.8), channel_id=1, source_target_pairs={{0,1},{1,0},{2,3},{3,2},{4,5},{5,4},{6,7},{7,6},{8,9},{9,8},{10,11... | collective-permute-start | bytes 6291464 | tf_op jit(solution)/shard_map/ppermute | solution.py:155
  18.7 1.4 copy-start.11
  18.7 2.0 copy-start.12
  18.7 2.0 copy-start.18
  18.7 2.0 copy-start.19
  22.4 70.6 %copy-start.2 = (bf16[16,256]{1,0:T(8,128)(2,1)S(1)}, bf16[16,256]{1,0:T(8,128)(2,1)}, u32[]{:S(2)}) copy-start(bf16[16,256]{1,0:T(8,128)(2,1)} %second_ref.1) | copy-start | bytes 24580
  22.4 70.6 %copy-start.3 = (f32[512]{0:T(512)S(1)}, f32[512]{0:T(512)}, u32[]{:S(2)}) copy-start(f32[512]{0:T(512)} %param.25) | copy-start | bytes 6148
  22.5 70.6 %copy-start.4 = (f32[256]{0:T(256)S(1)}, f32[256]{0:T(256)}, u32[]{:S(2)}) copy-start(f32[256]{0:T(256)} %param.23) | copy-start | bytes 3076
  139.9 2.0 copy-start.5
  141.9 10.3 %copy-start.13 = (f32[1024]{0:T(1024)S(1)}, f32[1024]{0:T(1024)}, u32[]{:S(2)}) copy-start(f32[1024]{0:T(1024)} %param.27) | copy-start | bytes 12292
  143.4 4.4 %collective-permute-start.1 = (bf16[1024,1024]{1,0:T(8,128)(2,1)}, bf16[1024,1024]{1,0:T(8,128)(2,1)S(1)}, u32[]{:S(2)}, u32[]{:S(2)}) collective-permute-start(bf16[1024,1024]{1,0:T(8,128)(2,1)} %constant_dynamic-slice_fusion.3), channel_id=1, source_target_pairs={{0,1},{1,0},{2,3},{3,2},{4,5},{5,4},{6,7},{7,6},{8,9},{9,8},{10,11... | collective-permute-start | bytes 6291464 | tf_op jit(solution)/shard_map/ppermute | solution.py:169
  143.4 8.7 %copy-start.6 = (bf16[1024,2048]{1,0:T(8,128)(2,1)S(1)}, bf16[1024,2048]{1,0:T(8,128)(2,1)}, u32[]{:S(2)}) copy-start(bf16[1024,2048]{1,0:T(8,128)(2,1)} %copy-done.5) | copy-start | bytes 12582916
  147.8 4.3 %copy-start.7 = (bf16[1024,1024]{1,0:T(8,128)(2,1)}, bf16[1024,1024]{1,0:T(8,128)(2,1)S(1)}, u32[]{:S(2)}) copy-start(bf16[1024,1024]{1,0:T(8,128)(2,1)S(1)} %collective-permute-done.1) | copy-start | bytes 6291460
  150.9 1.2 collective-permute-start.2
  155.5 4.2 %collective-permute-start.3 = (bf16[1024,1024]{1,0:T(8,128)(2,1)S(1)}, bf16[1024,1024]{1,0:T(8,128)(2,1)S(1)}, u32[]{:S(2)}, u32[]{:S(2)}) collective-permute-start(bf16[1024,1024]{1,0:T(8,128)(2,1)S(1)} %add_convert_fusion.2), channel_id=1, source_target_pairs={{0,1},{1,0},{2,3},{3,2},{4,5},{5,4},{6,7},{7,6},{8,9},{9,8},{10,11... | collective-permute-start | bytes 6291464 | tf_op jit(solution)/shard_map/ppermute | solution.py:155
  161.3 1.3 copy-start.9
  161.3 87.9 %copy-start.20 = (f32[2048]{0:T(1024)S(1)}, f32[2048]{0:T(1024)}, u32[]{:S(2)}) copy-start(f32[2048]{0:T(1024)} %param.28) | copy-start | bytes 24580
  249.3 9.5 %copy-start.10 = (bf16[1024,1024]{1,0:T(8,128)(2,1)S(1)}, bf16[1024,1024]{1,0:T(8,128)(2,1)}, u32[]{:S(2)}) copy-start(bf16[1024,1024]{1,0:T(8,128)(2,1)} %copy-done.9) | copy-start | bytes 6291460
  249.3 9.5 %copy-start.16 = (bf16[4096,1024]{1,0:T(8,128)(2,1)S(1)}, bf16[4096,1024]{1,0:T(8,128)(2,1)}, u32[]{:S(2)}) copy-start(bf16[4096,1024]{1,0:T(8,128)(2,1)} %all-gather.9.cloned.1.call-done) | copy-start | bytes 25165828
  384.5 10.7 %copy-start.17 = (bf16[1024,4096]{1,0:T(8,128)(2,1)S(1)}, bf16[1024,4096]{1,0:T(8,128)(2,1)}, u32[]{:S(2)}) copy-start(bf16[1024,4096]{1,0:T(8,128)(2,1)} %all-gather.11.cloned.1.call-done) | copy-start | bytes 25165828
  384.5 10.7 %copy-start.21 = (bf16[1024,1024]{1,0:T(8,128)(2,1)S(1)}, bf16[1024,1024]{1,0:T(8,128)(2,1)}, u32[]{:S(2)}) copy-start(bf16[1024,1024]{1,0:T(8,128)(2,1)} %multiply_convert_fusion.1) | copy-start | bytes 6291460
  402.1 6.5 %copy-start.14 = (f32[1024]{0:T(1024)S(1)}, f32[1024]{0:T(1024)}, u32[]{:S(2)}) copy-start(f32[1024]{0:T(1024)} %param.31) | copy-start | bytes 12292
  402.4 4.2 %collective-permute-start.4 = (bf16[1024,1024]{1,0:T(8,128)(2,1)S(1)}, bf16[1024,1024]{1,0:T(8,128)(2,1)S(1)}, u32[]{:S(2)}, u32[]{:S(2)}) collective-permute-start(bf16[1024,1024]{1,0:T(8,128)(2,1)S(1)} %constant_dynamic-slice_fusion), channel_id=1, source_target_pairs={{0,1},{1,0},{2,3},{3,2},{4,5},{5,4},{6,7},{7,6},{8,9},{9,8},{10,11... | collective-permute-start | bytes 6291464 | tf_op jit(solution)/shard_map/ppermute | solution.py:169
  407.4 1.2 collective-permute-start.5
  408.6 2.4 copy-start.1
Sparse Core Ops, SparseCore 0:
  9.5 75.5 all-gather.4
  87.1 48.8 all-gather.6
  138.7 110.4 all-gather.8
  251.8 132.6 all-gather.10
